TPU v7x, 32 devices: a whole 2x2x4 slice. The times are simulated.
32 devices in a mesh: sp: 8 (over z, x), tp: 4 (over y, core).
Axes of the slice: x: 2, y: 2, z: 4, core: 2. Of those that a mesh axis runs over, the one named last changes fastest.
Arguments:
- stream: bfloat16 [4096, 2048], P(('sp', 'tp')), may hold values from -6 to 6
- pool_in: bfloat16 [4096, 1024], P('sp', 'tp'), may hold values from -6 to 6
- doc_ids: int32 [4096], P('sp'), may hold values from 0 to 7, never falling along the last dimension, each value on 1 to 1024 neighbouring positions
- pool_map: bfloat16 [4, 256, 512], P('tp'), may hold values from -0.375 to 0.375
- pool_scale: float32 [2048], P('tp'), may hold values from 0.1 to 1.9
- out_weight: bfloat16 [2048, 2048], P('tp'), may hold values from -0.125 to 0.125
- norm_gain: float32 [2048], replicated, may hold values from 0.1 to 1.9
- routes: int32 [4096, 2], P('sp'), may hold values from 0 to 7, all different within a row; in each aligned block of 128 rows (0 to 127, 128 to 255, ...) at most 48 rows name the same one
- route_weight: float32 [4096, 2], P(('sp', 'tp')), may hold values from 0.2 to 1
- expert_gate: bfloat16 [8, 2048, 1024], P('sp', None, 'tp'), may hold values from -0.125 to 0.125
- expert_up: bfloat16 [8, 2048, 1024], P('sp', None, 'tp'), may hold values from -0.125 to 0.125
- expert_down: bfloat16 [8, 1024, 2048], P('sp', 'tp'), may hold values from -0.1875 to 0.1875
Outputs:
- result: bfloat16 [4096, 2048], P(('sp', 'tp'))
Inputs may be any that keep to these rules, and one draw needn't show every extreme that they name: `routes`: each token names 2 different experts; in each aligned block of 128 rows no expert is named by more than 48 rows, a bound that some block reaches. `doc_ids`: never falling; each document holds at most 1024 positions.
All inputs are finite; a program needn't handle non-finite values.
Results may differ from a plain program's by a relative error of at most 0.014.
Values may be sent and summed in bfloat16 or wider, within the bound.
A program may use at most 64 MiB of HBM per device.

v0:
```python
import functools

import jax
import jax.numpy as jnp
from jax import lax
from jax.experimental import pallas as pl
from jax.experimental.pallas import tpu as pltpu
from jax.sharding import PartitionSpec as P

HALO = 16
COLS = 512
PIECE = 256
EPS = 1e-06
MESH = pl.DeviceIdType.MESH
F32 = jnp.float32
BF16 = jnp.bfloat16


def flipped(index, mask):
    bit = 1
    while bit <= mask:
        if mask & bit:
            index = index + bit - 2 * bit * (index // bit % 2)
        bit *= 2
    return index


def window_sums(prior, prior_docs, own, own_docs, window):
    width = own.shape[1]
    ext_docs = jnp.concatenate([prior_docs, own_docs], axis=0)
    total = jnp.concatenate([prior, own], axis=0)
    counts = jnp.ones(ext_docs.shape, F32)
    step = 1
    while step < HALO:
        keep = (pltpu.roll(ext_docs, step, 0) == ext_docs) & (step < window)
        counts = counts + jnp.where(keep, pltpu.roll(counts, step, 0), 0.0)
        keep_wide = jnp.concatenate([keep.astype(F32)] * (width // 128), axis=1) > 0.5
        total = total + jnp.where(keep_wide, pltpu.roll(total, step, 0), 0.0)
        step *= 2
    counts_wide = jnp.concatenate([counts] * (width // 128), axis=1)
    return (total[HALO:] / counts_wide[HALO:] - own).astype(BF16)


def kernel(
    n_sp, n_tp, quarter, capacity, top,
    stream, pool_in, docs_row, pool_map, pool_scale, out_weight, gain, routes, weights,
    gate, up, down,
    out,
    gates, ups, downs, outw, halo, halo_docs, branch, partial, pair_send, pair_recv,
    far_send, far_recv, mixed, dispatch, arrived, crossed, hidden, hidden_send,
    answers, returned, docs,
    local_sem, halo_ssem, halo_rsem, g_ssem, g_rsem, w_ssem, w_rsem, n_ssem, f_ssem,
    p_ssem, p_rsem, y_ssem, y_rsem, d_ssem, d_rsem, c_ssem, c_rsem, h_ssem, h_rsem,
    r_ssem, r_rsem,
):
    sp, tp = lax.axis_index("sp"), lax.axis_index("tp")
    n_chip = n_tp // 2
    chip, parity = tp // 2, tp % 2
    other = 1 - parity
    partner = chip * 2 + other
    rows = pool_in.shape[0]
    width = stream.shape[1]
    ff = gate.shape[1]
    slots = n_sp * capacity
    half = n_sp // 2
    team, member = sp // half, sp % half
    span = half // 2
    chunks = width // COLS
    pieces = width // PIECE
    others = range(1, n_chip)

    def same(m):
        return (chip + m) % n_chip * 2 + parity

    def remote(src, dst, ssem, rsem, to):
        return pltpu.make_async_remote_copy(
            src_ref=src, dst_ref=dst, send_sem=ssem, recv_sem=rsem,
            device_id=to, device_id_type=MESH,
        )

    def peer(at):
        if at < half:
            return (1 - team) * half + flipped(member, at)
        return team * half + flipped(member, at - half)

    def cols(c):
        return pl.ds(c * COLS, COLS)

    def wide(p):
        return pl.ds(p * PIECE, PIECE)

    def block(e):
        return pl.ds(pl.multiple_of(e * capacity, 16), capacity)

    def owned(q):
        return pl.ds(pl.multiple_of(q * quarter, quarter), quarter)

    own_copies = [
        pltpu.make_async_copy(out_weight, outw, local_sem.at[0]),
        pltpu.make_async_copy(gate, gates.at[:, pl.ds(0, ff)], local_sem.at[1]),
        pltpu.make_async_copy(up, ups.at[:, pl.ds(0, ff)], local_sem.at[2]),
        pltpu.make_async_copy(down, downs.at[pl.ds(0, ff)], local_sem.at[3]),
    ]
    for c in own_copies:
        c.start()

    barrier = pltpu.get_barrier_semaphore()
    for d in range(1, n_sp):
        pl.semaphore_signal(barrier, inc=1, device_id=((sp + d) % n_sp, tp), device_id_type=MESH)
    pl.semaphore_signal(barrier, inc=1, device_id=(sp, partner), device_id_type=MESH)
    for m in others:
        pl.semaphore_signal(barrier, inc=1, device_id=(sp, same(m)), device_id_type=MESH)

    docs[...] = jnp.transpose(jnp.broadcast_to(docs_row[...].astype(F32), (128, rows)))
    window = jnp.left_shift(jnp.int32(2), tp)
    group_width = pool_in.shape[1]
    pooled = window_sums(
        jnp.zeros((HALO, group_width), F32), jnp.full((HALO, 128), -1.0, F32),
        pool_in[...].astype(F32), docs[...], window,
    )
    branch[...] = (
        jnp.dot(pooled, pool_map[...], preferred_element_type=F32) * pool_scale[...]
    ).astype(BF16)
    own_copies[0].wait()
    for c in range(chunks):
        partial[:, cols(c)] = jnp.dot(branch[...], outw[:, cols(c)], preferred_element_type=F32)

    def pair_owner(m):
        return (chip + m) % n_chip * 2 + other

    for m in range(n_chip):
        pair_send[m] = partial[owned(pair_owner(m)), :].astype(BF16)

    names = lax.broadcasted_iota(jnp.int32, (128, quarter), 0)
    own_routes = routes[:, owned(tp)]
    hots = [(own_routes[k : k + 1, :] == names).astype(F32) for k in range(top)]
    named = functools.reduce(lambda a, b: a + b, hots)
    above = (
        lax.broadcasted_iota(jnp.int32, (quarter, quarter), 0)
        < lax.broadcasted_iota(jnp.int32, (quarter, quarter), 1)
    ).astype(BF16)
    before = jnp.dot(named.astype(BF16), above, preferred_element_type=F32)
    slot_names = lax.broadcasted_iota(jnp.int32, (slots, quarter), 0)
    places = []
    for k in range(top):
        rank = jnp.sum(hots[k] * before, axis=0, keepdims=True).astype(jnp.int32)
        places.append((slot_names == own_routes[k : k + 1, :] * capacity + rank).astype(F32))
    spread = functools.reduce(lambda a, b: a + b, places).astype(BF16)
    picks = [jnp.transpose(p).astype(BF16) for p in places]
    scales = [
        jnp.transpose(jnp.broadcast_to(weights[k : k + 1, :], (128, quarter)))[:, :1]
        for k in range(top)
    ]

    pl.semaphore_wait(barrier, n_sp - 1 + 1 + n_chip - 1)

    right = ((sp + 1) % n_sp, tp)
    halo_copies = [
        remote(pool_in.at[pl.ds(rows - HALO, HALO)], halo, halo_ssem.at[0], halo_rsem.at[0], right),
        remote(docs.at[pl.ds(rows - HALO, HALO)], halo_docs, halo_ssem.at[1], halo_rsem.at[1], right),
    ]
    for c in halo_copies:
        c.start()

    def far_down(p, m):
        j = (n_chip - m) % n_chip
        return remote(
            down.at[:, wide(p)], downs.at[pl.ds(2 * j * ff, ff), wide(p)],
            w_ssem.at[m, p], w_rsem.at[2 * j, p], (sp, same(m)),
        )

    def near_down(p):
        return remote(
            down.at[:, wide(p)], downs.at[pl.ds(ff, ff), wide(p)],
            n_ssem.at[p], w_rsem.at[1, p], (sp, partner),
        )

    def forward_down(p, m):
        return remote(
            downs.at[pl.ds(2 * m * ff, ff), wide(p)],
            downs.at[pl.ds((2 * m + 1) * ff, ff), wide(p)],
            f_ssem.at[m, p], w_rsem.at[2 * m + 1, p], (sp, partner),
        )

    near_hidden = [
        remote(gate, gates.at[:, pl.ds(ff, ff)], g_ssem.at[0], g_rsem.at[0], (sp, partner)),
        remote(up, ups.at[:, pl.ds(ff, ff)], g_ssem.at[1], g_rsem.at[1], (sp, partner)),
    ]

    def send_down(*which):
        for p in which:
            for m in others:
                far_down(p, m).start()

    def pair_copy(m, c):
        return remote(
            pair_send.at[m, :, cols(c)], pair_recv.at[m, :, cols(c)],
            p_ssem.at[m, c], p_rsem.at[m, c], (sp, partner),
        )

    order = list(others) + [0]
    send_down(0)
    for m in order:
        @pl.when(pair_owner(m) != 0)
        def _(m=m):
            for c in range(chunks):
                pair_copy(m, c).start()

    for c in halo_copies:
        c.wait_recv()
    first = sp == 0
    head = window_sums(
        jnp.where(first, 0.0, halo[...].astype(F32)), jnp.where(first, -1.0, halo_docs[...]),
        pool_in[pl.ds(0, HALO), :].astype(F32), docs[pl.ds(0, HALO), :], window,
    )
    head = (jnp.dot(head, pool_map[...], preferred_element_type=F32) * pool_scale[...]).astype(BF16)
    head = jnp.dot(head, outw[...], preferred_element_type=F32)
    partial[pl.ds(0, HALO), :] = head
    for m in order:
        @pl.when(pair_owner(m) == 0)
        def _(m=m):
            pair_send[m, pl.ds(0, HALO), :] = head.astype(BF16)
            for c in range(chunks):
                pair_copy(m, c).start()

    def far_copy(m, c):
        j = (n_chip - m) % n_chip
        return remote(
            far_send.at[m, :, cols(c)], far_recv.at[j, :, cols(c)],
            y_ssem.at[m, c], y_rsem.at[j, c], (sp, same(m)),
        )

    for m in others:
        for c in range(chunks):
            pair_copy(m, c).wait_recv()
            far_send[m, :, cols(c)] = (
                partial[owned(same(m)), cols(c)] + pair_recv[m, :, cols(c)].astype(F32)
            ).astype(BF16)
            far_copy(m, c).start()
    for c in near_hidden:
        c.start()
    for p in range(pieces):
        near_down(p).start()
    send_down(1, 2)

    everything = pl.ds(0, width)

    def outward(at, c=None):
        e = peer(at)
        columns = everything if c is None else cols(c)
        slot = c or 0
        return remote(
            dispatch.at[block(e), columns], arrived.at[pl.ds(at * capacity, capacity), columns],
            d_ssem.at[at, slot], d_rsem.at[at, slot], (e, tp),
        )

    for c in range(chunks):
        pair_copy(0, c).wait_recv()
        mine = partial[owned(tp), cols(c)] + pair_recv[0, :, cols(c)].astype(F32)
        for m in others:
            far_copy((n_chip - m) % n_chip, c).wait_recv()
            mine = mine + far_recv[m, :, cols(c)].astype(F32)
        mixed[:, cols(c)] = (stream[:, cols(c)].astype(F32) + mine).astype(BF16)
        dispatch[:, cols(c)] = jnp.dot(
            spread, mixed[:, cols(c)], preferred_element_type=F32
        ).astype(BF16)
        for at in range(span):
            outward(at, c).start()
    for at in list(range(half + 1, half + span)) + list(range(span, half)) + list(
        range(half + span, n_sp)
    ):
        outward(at).start()
    arrived[pl.ds(half * capacity, capacity), :] = dispatch[block(sp), :]

    size = span * capacity

    def places_of(g):
        return range(g * span, (g + 1) * span)

    def lines(g):
        return pl.ds(g * size, size)

    def gated(x):
        g = jnp.dot(x, gates[...], preferred_element_type=F32)
        u = jnp.dot(x, ups[...], preferred_element_type=F32)
        return (g / (1.0 + jnp.exp(-g)) * u).astype(BF16)

    def cross_copy(m, g):
        j = (n_chip - m) % n_chip
        return remote(
            crossed.at[0, lines(g)], crossed.at[j, lines(g)],
            c_ssem.at[m, g], c_rsem.at[j, g], (sp, same(m)),
        )

    def hidden_copy(j, g):
        m = (n_chip - j) % n_chip
        return remote(
            hidden_send.at[j - 1, lines(g)], hidden.at[lines(g), pl.ds(2 * m * ff, 2 * ff)],
            h_ssem.at[j, g], h_rsem.at[m, g], (sp, same(j)),
        )

    def normalize(g):
        for at in places_of(g):
            if at < span:
                for c in range(chunks):
                    outward(at, c).wait_recv()
            elif at != half:
                outward(at).wait_recv()
        value = arrived[lines(g), :].astype(F32)
        crossed[0, lines(g), :] = (
            value * lax.rsqrt(jnp.mean(value * value, axis=1, keepdims=True) + EPS) * gain[...]
        ).astype(BF16)
        for m in others:
            cross_copy(m, g).start()

    ready = []

    def own_hidden(g):
        if not ready:
            ready.append(True)
            for c in own_copies[1:3]:
                c.wait()
            for c in near_hidden:
                c.wait_recv()
        hidden[lines(g), pl.ds(0, 2 * ff)] = gated(crossed[0, lines(g), :])

    def far_hidden(g):
        for j in others:
            cross_copy((n_chip - j) % n_chip, g).wait_recv()
            hidden_send[j - 1, lines(g), :] = gated(crossed[j, lines(g), :])
            hidden_copy(j, g).start()

    held = set()

    def pass_down(*which):
        for p in which:
            for m in others:
                j = (n_chip - m) % n_chip
                far_down(p, j).wait_recv()
                forward_down(p, m).start()

    def homeward(at, p):
        e = peer(at)
        return remote(
            answers.at[pl.ds(at * capacity, capacity), wide(p)], returned.at[block(sp), wide(p)],
            r_ssem.at[at, p], r_rsem.at[at, p], (e, tp),
        )

    def answer(g, *which):
        if ("hidden", g) not in held:
            held.add(("hidden", g))
            for m in others:
                hidden_copy((n_chip - m) % n_chip, g).wait_recv()
        for p in which:
            if p not in held:
                if not held & set(range(pieces)):
                    own_copies[3].wait()
                held.add(p)
                near_down(p).wait_recv()
                for m in others:
                    forward_down(p, m).wait_recv()
            answers[lines(g), wide(p)] = jnp.dot(
                hidden[lines(g), :], downs[:, wide(p)], preferred_element_type=F32
            ).astype(BF16)
            for at in places_of(g):
                if at == half:
                    returned[block(sp), wide(p)] = answers[pl.ds(at * capacity, capacity), wide(p)]
                else:
                    homeward(at, p).start()

    early = tuple(range(pieces - 3))
    late = tuple(range(pieces - 3, pieces))
    normalize(2)
    own_hidden(2)
    normalize(0)
    send_down(*early[3:])
    own_hidden(0)
    far_hidden(2)
    far_hidden(0)
    send_down(late[0])
    pass_down(*early)
    answer(0, *early)
    normalize(1)
    send_down(*late[1:])
    own_hidden(1)
    answer(2, *early)
    far_hidden(1)
    normalize(3)
    own_hidden(3)
    pass_down(*late)
    answer(1, *early)
    answer(0, *late)
    answer(1, *late)
    answer(2, *late)
    far_hidden(3)
    answer(3, *range(pieces))

    for p in range(pieces):
        for at in range(n_sp):
            if at != half:
                homeward(at, p).wait_recv()
        result = mixed[:, wide(p)].astype(F32)
        for k in range(top):
            result = result + scales[k] * jnp.dot(
                picks[k], returned[:, wide(p)], preferred_element_type=F32
            )
        out[:, wide(p)] = result.astype(BF16)

    for c in halo_copies + near_hidden:
        c.wait_send()
    for m in range(n_chip):
        for c in range(chunks):
            pair_copy(m, c).wait_send()
    for p in range(pieces):
        near_down(p).wait_send()
        for m in others:
            far_down(p, m).wait_send()
            forward_down(p, m).wait_send()
    for m in others:
        for c in range(chunks):
            far_copy(m, c).wait_send()
        for g in range(4):
            cross_copy(m, g).wait_send()
            hidden_copy(m, g).wait_send()
    for at in range(n_sp):
        if at == half:
            continue
        if at < span:
            for c in range(chunks):
                outward(at, c).wait_send()
        else:
            outward(at).wait_send()
        for p in range(pieces):
            homeward(at, p).wait_send()


def per_device(
    n_sp, n_tp,
    stream, pool_in, doc_ids, pool_map, pool_scale, out_weight, norm_gain, routes, route_weight,
    expert_gate, expert_up, expert_down,
):
    rows, group_width = pool_in.shape
    quarter, width = stream.shape
    top = routes.shape[1]
    ff = expert_gate.shape[2]
    capacity = max(2, 3 * top * quarter // (2 * n_sp))
    capacity = -(-capacity // 16) * 16
    slots = n_sp * capacity
    n_chip = n_tp // 2
    vmem = pl.BlockSpec(memory_space=pltpu.VMEM)
    hbm = pl.BlockSpec(memory_space=pl.ANY)
    dma = pltpu.SemaphoreType.DMA
    V = pltpu.VMEM
    branch_width = out_weight.shape[0]
    chunks = width // COLS
    pieces = width // PIECE
    return pl.pallas_call(
        functools.partial(kernel, n_sp, n_tp, quarter, capacity, top),
        out_shape=jax.ShapeDtypeStruct((quarter, width), BF16),
        in_specs=[vmem] * 5 + [hbm] + [vmem] * 3 + [hbm] * 3,
        out_specs=vmem,
        scratch_shapes=[
            V((width, 2 * ff), BF16),
            V((width, 2 * ff), BF16),
            V((n_tp * ff, width), BF16),
            V((branch_width, width), BF16),
            V((HALO, group_width), BF16),
            V((HALO, 128), F32),
            V((rows, branch_width), BF16),
            V((rows, width), F32),
            V((n_chip, quarter, width), BF16),
            V((n_chip, quarter, width), BF16),
            V((n_chip, quarter, width), BF16),
            V((n_chip, quarter, width), BF16),
            V((quarter, width), BF16),
            V((slots, width), BF16),
            V((slots, width), BF16),
            V((n_chip, slots, width), BF16),
            V((slots, n_tp * ff), BF16),
            V((n_chip - 1, slots, 2 * ff), BF16),
            V((slots, width), BF16),
            V((slots, width), BF16),
            V((rows, 128), F32),
            dma((4,)),
            dma((2,)),
            dma((2,)),
            dma((2,)),
            dma((2,)),
            dma((n_chip, pieces)),
            dma((n_tp, pieces)),
            dma((pieces,)),
            dma((n_chip, pieces)),
            dma((n_chip, chunks)),
            dma((n_chip, chunks)),
            dma((n_chip, chunks)),
            dma((n_chip, chunks)),
            dma((n_sp, chunks)),
            dma((n_sp, chunks)),
            dma((n_chip, 4)),
            dma((n_chip, 4)),
            dma((n_chip, 4)),
            dma((n_chip, 4)),
            dma((n_sp, pieces)),
            dma((n_sp, pieces)),
        ],
        compiler_params=pltpu.CompilerParams(
            collective_id=0, has_side_effects=True, vmem_limit_bytes=60 * 1024 * 1024
        ),
    )(
        stream, pool_in, doc_ids[None, :], pool_map[0],
        pool_scale[None, :], out_weight, norm_gain[None, :], routes.T, route_weight.T,
        expert_gate[0], expert_up[0], expert_down[0],
    )


def solution(mesh):
    in_specs = (
        P(("sp", "tp"), None),
        P("sp", "tp"),
        P("sp"),
        P("tp", None, None),
        P("tp"),
        P("tp", None),
        P(),
        P("sp", None),
        P(("sp", "tp"), None),
        P("sp", None, "tp"),
        P("sp", None, "tp"),
        P("sp", "tp", None),
    )
    out_specs = P(("sp", "tp"), None)
    return jax.shard_map(
        functools.partial(per_device, mesh.shape["sp"], mesh.shape["tp"]),
        mesh=mesh, in_specs=in_specs, out_specs=out_specs, check_vma=False,
    )
```

profile of v0, /device:TPU:0, one launch (start us, length us, event | category | flops | bytes accessed | tf_op | source)
XLA Modules:
  0.0 108.6 jit_solution(7733407021698215501)
XLA Ops:
  0.0 106.7 %shard_map.118 = bf16[128,2048]{1,0:T(8,128)(2,1)} custom-call(bf16[128,2048]{1,0:T(8,128)(2,1)} %stream.1, bf16[512,256]{1,0:T(8,128)(2,1)} %pool_in.1, s32[1,512]{1,0:T(1,128)} %bitcast.15, bf16[256,512]{1,0:T(8,128)(2,1)} %bitcast.12, f32[1,512]{1,0:T(1,128)} %bitcast.16, bf16[512,2048]{1,0:T(8,128)(2,1)} %out_weight.1, f32[1,2048]{1,0:T(1,128)} %bitcast.13, ...), custom_call_target="tpu_custom_call" | custom-call | tf_op jit(solution)/shard_map/pallas_call | solution.py:457
  106.7 1.9 %copy.14 = bf16[128,2048]{1,0:T(8,128)(2,1)} copy(bf16[128,2048]{1,0:T(8,128)(2,1)} %shard_map.118) | data formatting | bytes 1048576
where the time goes:
time: 109 us
  Pallas kernels  107 us (98%)
  local copies, waits for them, and re-layouts  1.88 us (2%)
    pallas_call x1, Pallas kernels, per_device(): pl.pallas_call(functools.partial(kernel, n_sp, n_tp, quarter, capacity, t...  107 us

commit v1 on v0

--- a/solution.py
+++ b/solution.py
@@ -48,10 +48,10 @@
     out,
     gates, ups, downs, outw, halo, halo_docs, branch, partial, pair_send, pair_recv,
     far_send, far_recv, mixed, dispatch, arrived, crossed, hidden, hidden_send,
-    answers, returned, docs,
+    answers, returned, mixed_sib, dispatch_sib, docs, map_here, stream_here, out_here,
     local_sem, halo_ssem, halo_rsem, g_ssem, g_rsem, w_ssem, w_rsem, n_ssem, f_ssem,
     p_ssem, p_rsem, y_ssem, y_rsem, d_ssem, d_rsem, c_ssem, c_rsem, h_ssem, h_rsem,
-    r_ssem, r_rsem,
+    r_ssem, r_rsem, out_sem, a_ssem, a_rsem, s_ssem, s_rsem,
 ):
     sp, tp = lax.axis_index("sp"), lax.axis_index("tp")
     n_chip = n_tp // 2
@@ -95,15 +95,6 @@
     def owned(q):
         return pl.ds(pl.multiple_of(q * quarter, quarter), quarter)
 
-    own_copies = [
-        pltpu.make_async_copy(out_weight, outw, local_sem.at[0]),
-        pltpu.make_async_copy(gate, gates.at[:, pl.ds(0, ff)], local_sem.at[1]),
-        pltpu.make_async_copy(up, ups.at[:, pl.ds(0, ff)], local_sem.at[2]),
-        pltpu.make_async_copy(down, downs.at[pl.ds(0, ff)], local_sem.at[3]),
-    ]
-    for c in own_copies:
-        c.start()
-
     barrier = pltpu.get_barrier_semaphore()
     for d in range(1, n_sp):
         pl.semaphore_signal(barrier, inc=1, device_id=((sp + d) % n_sp, tp), device_id_type=MESH)
@@ -111,109 +102,110 @@
     for m in others:
         pl.semaphore_signal(barrier, inc=1, device_id=(sp, same(m)), device_id_type=MESH)
 
+    own_copies = [
+        pltpu.make_async_copy(out_weight, outw, local_sem.at[0]),
+        pltpu.make_async_copy(gate, gates.at[:, pl.ds(0, ff)], local_sem.at[1]),
+        pltpu.make_async_copy(up, ups.at[:, pl.ds(0, ff)], local_sem.at[2]),
+        pltpu.make_async_copy(down, downs.at[pl.ds(0, ff)], local_sem.at[3]),
+        pltpu.make_async_copy(pool_map, map_here, local_sem.at[4]),
+        pltpu.make_async_copy(stream, stream_here, local_sem.at[5]),
+    ]
+    for at in (4, 0, 1, 2, 3, 5):
+        own_copies[at].start()
+
     docs[...] = jnp.transpose(jnp.broadcast_to(docs_row[...].astype(F32), (128, rows)))
+    pl.semaphore_wait(barrier, n_sp - 1 + 1 + n_chip - 1)
+
+    right = ((sp + 1) % n_sp, tp)
+    halo_copies = [
+        remote(pool_in.at[pl.ds(rows - HALO, HALO)], halo, halo_ssem.at[0], halo_rsem.at[0], right),
+        remote(docs.at[pl.ds(rows - HALO, HALO)], halo_docs, halo_ssem.at[1], halo_rsem.at[1], right),
+    ]
+
+    @pl.when(sp != n_sp - 1)
+    def _():
+        for c in halo_copies:
+            c.start()
+
+    @pl.when(sp == 0)
+    def _():
+        halo[...] = jnp.zeros_like(halo)
+        halo_docs[...] = jnp.full_like(halo_docs, -1.0)
+
+
+    def far_down(p, m):
+        j = (n_chip - m) % n_chip
+        return remote(
+            down.at[:, wide(p)], downs.at[pl.ds(2 * j * ff, ff), wide(p)],
+            w_ssem.at[m, p], w_rsem.at[2 * j, p], (sp, same(m)),
+        )
+
+    def near_down(p):
+        return remote(
+            down.at[:, wide(p)], downs.at[pl.ds(ff, ff), wide(p)],
+            n_ssem.at[p], w_rsem.at[1, p], (sp, partner),
+        )
+
+    def forward_down(p, m):
+        return remote(
+            downs.at[pl.ds(2 * m * ff, ff), wide(p)],
+            downs.at[pl.ds((2 * m + 1) * ff, ff), wide(p)],
+            f_ssem.at[m, p], w_rsem.at[2 * m + 1, p], (sp, partner),
+        )
+
+    near_hidden = [
+        remote(gate, gates.at[:, pl.ds(ff, ff)], g_ssem.at[0], g_rsem.at[0], (sp, partner)),
+        remote(up, ups.at[:, pl.ds(ff, ff)], g_ssem.at[1], g_rsem.at[1], (sp, partner)),
+    ]
+
+    def send_down(*which):
+        for p in which:
+            for m in others:
+                far_down(p, m).start()
+
+    send_down(0, 1)
+
     window = jnp.left_shift(jnp.int32(2), tp)
     group_width = pool_in.shape[1]
     pooled = window_sums(
         jnp.zeros((HALO, group_width), F32), jnp.full((HALO, 128), -1.0, F32),
         pool_in[...].astype(F32), docs[...], window,
     )
+    own_copies[4].wait()
     branch[...] = (
-        jnp.dot(pooled, pool_map[...], preferred_element_type=F32) * pool_scale[...]
+        jnp.dot(pooled, map_here[...], preferred_element_type=F32) * pool_scale[...]
     ).astype(BF16)
     own_copies[0].wait()
+
+    def pair_owner(m):
+        return (chip + m) % n_chip * 2 + other
+
+    def pair_copy(m, c):
+        return remote(
+            pair_send.at[m, :, cols(c)], pair_recv.at[m, :, cols(c)],
+            p_ssem.at[m, c], p_rsem.at[m, c], (sp, partner),
+        )
+
+    order = list(others) + [0]
     for c in range(chunks):
         partial[:, cols(c)] = jnp.dot(branch[...], outw[:, cols(c)], preferred_element_type=F32)
-
-    def pair_owner(m):
-        return (chip + m) % n_chip * 2 + other
-
-    for m in range(n_chip):
-        pair_send[m] = partial[owned(pair_owner(m)), :].astype(BF16)
-
-    names = lax.broadcasted_iota(jnp.int32, (128, quarter), 0)
-    own_routes = routes[:, owned(tp)]
-    hots = [(own_routes[k : k + 1, :] == names).astype(F32) for k in range(top)]
-    named = functools.reduce(lambda a, b: a + b, hots)
-    above = (
-        lax.broadcasted_iota(jnp.int32, (quarter, quarter), 0)
-        < lax.broadcasted_iota(jnp.int32, (quarter, quarter), 1)
-    ).astype(BF16)
-    before = jnp.dot(named.astype(BF16), above, preferred_element_type=F32)
-    slot_names = lax.broadcasted_iota(jnp.int32, (slots, quarter), 0)
-    places = []
-    for k in range(top):
-        rank = jnp.sum(hots[k] * before, axis=0, keepdims=True).astype(jnp.int32)
-        places.append((slot_names == own_routes[k : k + 1, :] * capacity + rank).astype(F32))
-    spread = functools.reduce(lambda a, b: a + b, places).astype(BF16)
-    picks = [jnp.transpose(p).astype(BF16) for p in places]
-    scales = [
-        jnp.transpose(jnp.broadcast_to(weights[k : k + 1, :], (128, quarter)))[:, :1]
-        for k in range(top)
-    ]
-
-    pl.semaphore_wait(barrier, n_sp - 1 + 1 + n_chip - 1)
-
-    right = ((sp + 1) % n_sp, tp)
-    halo_copies = [
-        remote(pool_in.at[pl.ds(rows - HALO, HALO)], halo, halo_ssem.at[0], halo_rsem.at[0], right),
-        remote(docs.at[pl.ds(rows - HALO, HALO)], halo_docs, halo_ssem.at[1], halo_rsem.at[1], right),
-    ]
-    for c in halo_copies:
-        c.start()
-
-    def far_down(p, m):
-        j = (n_chip - m) % n_chip
-        return remote(
-            down.at[:, wide(p)], downs.at[pl.ds(2 * j * ff, ff), wide(p)],
-            w_ssem.at[m, p], w_rsem.at[2 * j, p], (sp, same(m)),
-        )
-
-    def near_down(p):
-        return remote(
-            down.at[:, wide(p)], downs.at[pl.ds(ff, ff), wide(p)],
-            n_ssem.at[p], w_rsem.at[1, p], (sp, partner),
-        )
-
-    def forward_down(p, m):
-        return remote(
-            downs.at[pl.ds(2 * m * ff, ff), wide(p)],
-            downs.at[pl.ds((2 * m + 1) * ff, ff), wide(p)],
-            f_ssem.at[m, p], w_rsem.at[2 * m + 1, p], (sp, partner),
-        )
-
-    near_hidden = [
-        remote(gate, gates.at[:, pl.ds(ff, ff)], g_ssem.at[0], g_rsem.at[0], (sp, partner)),
-        remote(up, ups.at[:, pl.ds(ff, ff)], g_ssem.at[1], g_rsem.at[1], (sp, partner)),
-    ]
-
-    def send_down(*which):
-        for p in which:
-            for m in others:
-                far_down(p, m).start()
-
-    def pair_copy(m, c):
-        return remote(
-            pair_send.at[m, :, cols(c)], pair_recv.at[m, :, cols(c)],
-            p_ssem.at[m, c], p_rsem.at[m, c], (sp, partner),
-        )
-
-    order = list(others) + [0]
-    send_down(0)
-    for m in order:
-        @pl.when(pair_owner(m) != 0)
-        def _(m=m):
-            for c in range(chunks):
+        for m in order:
+            pair_send[m, :, cols(c)] = partial[owned(pair_owner(m)), cols(c)].astype(BF16)
+
+            @pl.when(pair_owner(m) != 0)
+            def _(m=m, c=c):
                 pair_copy(m, c).start()
 
-    for c in halo_copies:
-        c.wait_recv()
-    first = sp == 0
+    @pl.when(sp != 0)
+    def _():
+        for c in halo_copies:
+            c.wait_recv()
+
     head = window_sums(
-        jnp.where(first, 0.0, halo[...].astype(F32)), jnp.where(first, -1.0, halo_docs[...]),
+        halo[...].astype(F32), halo_docs[...],
         pool_in[pl.ds(0, HALO), :].astype(F32), docs[pl.ds(0, HALO), :], window,
     )
-    head = (jnp.dot(head, pool_map[...], preferred_element_type=F32) * pool_scale[...]).astype(BF16)
+    head = (jnp.dot(head, map_here[...], preferred_element_type=F32) * pool_scale[...]).astype(BF16)
     head = jnp.dot(head, outw[...], preferred_element_type=F32)
     partial[pl.ds(0, HALO), :] = head
     for m in order:
@@ -237,11 +229,46 @@
                 partial[owned(same(m)), cols(c)] + pair_recv[m, :, cols(c)].astype(F32)
             ).astype(BF16)
             far_copy(m, c).start()
+    send_down(2)
     for c in near_hidden:
         c.start()
     for p in range(pieces):
         near_down(p).start()
-    send_down(1, 2)
+
+    names = lax.broadcasted_iota(jnp.int32, (128, quarter), 0)
+    above = (
+        lax.broadcasted_iota(jnp.int32, (quarter, quarter), 0)
+        < lax.broadcasted_iota(jnp.int32, (quarter, quarter), 1)
+    ).astype(BF16)
+    own_routes = routes[:, owned(tp)]
+
+    def ranked(block_routes, first_slot, count):
+        hots = [(block_routes[k : k + 1, :] == names).astype(F32) for k in range(top)]
+        named = functools.reduce(lambda a, b: a + b, hots)
+        before = jnp.dot(named.astype(BF16), above, preferred_element_type=F32)
+        slot_names = lax.broadcasted_iota(jnp.int32, (count, quarter), 0) + first_slot
+        places = []
+        for k in range(top):
+            rank = jnp.sum(hots[k] * before, axis=0, keepdims=True).astype(jnp.int32)
+            places.append(
+                (slot_names == block_routes[k : k + 1, :] * capacity + rank).astype(F32)
+            )
+        return places
+
+    places = ranked(own_routes, 0, slots)
+    spread = functools.reduce(lambda a, b: a + b, places).astype(BF16)
+    sib_spread = {
+        m: functools.reduce(
+            lambda a, b: a + b,
+            ranked(routes[:, owned(same(m))], team * half * capacity, half * capacity),
+        ).astype(BF16)
+        for m in others
+    }
+    picks = [jnp.transpose(p).astype(BF16) for p in places]
+    scales = [
+        jnp.transpose(jnp.broadcast_to(weights[k : k + 1, :], (128, quarter)))[:, :1]
+        for k in range(top)
+    ]
 
     everything = pl.ds(0, width)
 
@@ -254,22 +281,57 @@
             d_ssem.at[at, slot], d_rsem.at[at, slot], (e, tp),
         )
 
+    def chunked(at):
+        return at < span or half < at < half + span
+
+    def gather_copy(m, c):
+        j = (n_chip - m) % n_chip
+        return remote(
+            mixed.at[:, cols(c)], mixed_sib.at[j - 1, :, cols(c)],
+            a_ssem.at[m, c], a_rsem.at[j, c], (sp, same(m)),
+        )
+
+    def gather(*which):
+        for c in which:
+            for m in others:
+                gather_copy(m, c).start()
+
+    def sib_outward(m, at):
+        e = peer(at)
+        return remote(
+            dispatch_sib.at[m - 1, block(e - team * half)],
+            crossed.at[m, pl.ds(at * capacity, capacity)],
+            s_ssem.at[m, at], s_rsem.at[m, at], (e, tp),
+        )
+
+    own_copies[5].wait()
     for c in range(chunks):
         pair_copy(0, c).wait_recv()
         mine = partial[owned(tp), cols(c)] + pair_recv[0, :, cols(c)].astype(F32)
         for m in others:
             far_copy((n_chip - m) % n_chip, c).wait_recv()
             mine = mine + far_recv[m, :, cols(c)].astype(F32)
-        mixed[:, cols(c)] = (stream[:, cols(c)].astype(F32) + mine).astype(BF16)
+        mixed[:, cols(c)] = (stream_here[:, cols(c)].astype(F32) + mine).astype(BF16)
         dispatch[:, cols(c)] = jnp.dot(
             spread, mixed[:, cols(c)], preferred_element_type=F32
         ).astype(BF16)
-        for at in range(span):
-            outward(at, c).start()
-    for at in list(range(half + 1, half + span)) + list(range(span, half)) + list(
-        range(half + span, n_sp)
-    ):
-        outward(at).start()
+        for at in range(n_sp):
+            if chunked(at):
+                outward(at, c).start()
+    gather(0, 1, 2, 3)
+    outer = member // span == team
+    second, fourth = range(span, half), range(half + span, n_sp)
+
+    @pl.when(outer)
+    def _():
+        for at in list(fourth) + list(second):
+            outward(at).start()
+
+    @pl.when(jnp.logical_not(outer))
+    def _():
+        for at in list(second) + list(fourth):
+            outward(at).start()
+
     arrived[pl.ds(half * capacity, capacity), :] = dispatch[block(sp), :]
 
     size = span * capacity
@@ -299,19 +361,34 @@
             h_ssem.at[j, g], h_rsem.at[m, g], (sp, same(j)),
         )
 
+    def normed(x):
+        value = x.astype(F32)
+        return (
+            value * lax.rsqrt(jnp.mean(value * value, axis=1, keepdims=True) + EPS) * gain[...]
+        ).astype(BF16)
+
     def normalize(g):
         for at in places_of(g):
-            if at < span:
+            if chunked(at):
                 for c in range(chunks):
                     outward(at, c).wait_recv()
             elif at != half:
                 outward(at).wait_recv()
-        value = arrived[lines(g), :].astype(F32)
-        crossed[0, lines(g), :] = (
-            value * lax.rsqrt(jnp.mean(value * value, axis=1, keepdims=True) + EPS) * gain[...]
-        ).astype(BF16)
+        crossed[0, lines(g), :] = normed(arrived[lines(g), :])
+        if g < 2:
+            for m in others:
+                cross_copy(m, g).start()
+
+    def sib_dispatch():
         for m in others:
-            cross_copy(m, g).start()
+            for c in range(chunks):
+                gather_copy((n_chip - m) % n_chip, c).wait_recv()
+                dispatch_sib[m - 1, :, cols(c)] = jnp.dot(
+                    sib_spread[m], mixed_sib[m - 1, :, cols(c)], preferred_element_type=F32
+                ).astype(BF16)
+            for at in range(half + 1, n_sp):
+                sib_outward(m, at).start()
+            crossed[m, pl.ds(half * capacity, capacity), :] = dispatch_sib[m - 1, block(member), :]
 
     ready = []
 
@@ -326,8 +403,15 @@
 
     def far_hidden(g):
         for j in others:
-            cross_copy((n_chip - j) % n_chip, g).wait_recv()
-            hidden_send[j - 1, lines(g), :] = gated(crossed[j, lines(g), :])
+            if g < 2:
+                cross_copy((n_chip - j) % n_chip, g).wait_recv()
+                x = crossed[j, lines(g), :]
+            else:
+                for at in places_of(g):
+                    if at != half:
+                        sib_outward(j, at).wait_recv()
+                x = normed(crossed[j, lines(g), :])
+            hidden_send[j - 1, lines(g), :] = gated(x)
             hidden_copy(j, g).start()
 
     held = set()
@@ -368,45 +452,55 @@
                 else:
                     homeward(at, p).start()
 
-    early = tuple(range(pieces - 3))
-    late = tuple(range(pieces - 3, pieces))
     normalize(2)
     own_hidden(2)
     normalize(0)
-    send_down(*early[3:])
+    send_down(3)
     own_hidden(0)
-    far_hidden(2)
+    sib_dispatch()
+    pass_down(0, 1, 2)
     far_hidden(0)
-    send_down(late[0])
-    pass_down(*early)
-    answer(0, *early)
+    send_down(4)
     normalize(1)
-    send_down(*late[1:])
+    send_down(5)
     own_hidden(1)
-    answer(2, *early)
-    far_hidden(1)
+    answer(0, 0, 1, 2)
+    pass_down(3)
+    answer(0, 3)
     normalize(3)
     own_hidden(3)
-    pass_down(*late)
-    answer(1, *early)
-    answer(0, *late)
-    answer(1, *late)
-    answer(2, *late)
+    far_hidden(2)
+    far_hidden(1)
     far_hidden(3)
-    answer(3, *range(pieces))
-
-    for p in range(pieces):
-        for at in range(n_sp):
-            if at != half:
-                homeward(at, p).wait_recv()
-        result = mixed[:, wide(p)].astype(F32)
-        for k in range(top):
-            result = result + scales[k] * jnp.dot(
-                picks[k], returned[:, wide(p)], preferred_element_type=F32
-            )
-        out[:, wide(p)] = result.astype(BF16)
-
-    for c in halo_copies + near_hidden:
+    send_down(6, 7)
+    pass_down(4)
+    answer(0, 4)
+    answer(1, 0, 1, 2, 3, 4)
+    pass_down(5)
+    answer(0, 5)
+    answer(1, 5)
+    answer(2, 0, 1, 2, 3, 4, 5)
+    pass_down(6)
+    answer(0, 6)
+    answer(1, 6)
+    answer(3, 0, 1, 2, 3, 4, 5, 6)
+    pass_down(7)
+    answer(0, 7)
+    answer(1, 7)
+    answer(2, 6, 7)
+    answer(3, 7)
+
+    def out_copy(p):
+        return pltpu.make_async_copy(
+            out_here.at[:, wide(p)], out.at[:, wide(p)], out_sem.at[p]
+        )
+
+    @pl.when(sp != n_sp - 1)
+    def _():
+        for c in halo_copies:
+            c.wait_send()
+
+    for c in near_hidden:
         c.wait_send()
     for m in range(n_chip):
         for c in range(chunks):
@@ -419,19 +513,39 @@
     for m in others:
         for c in range(chunks):
             far_copy(m, c).wait_send()
+            gather_copy(m, c).wait_send()
         for g in range(4):
-            cross_copy(m, g).wait_send()
+            if g < 2:
+                cross_copy(m, g).wait_send()
             hidden_copy(m, g).wait_send()
+        for at in range(half + 1, n_sp):
+            sib_outward(m, at).wait_send()
     for at in range(n_sp):
         if at == half:
             continue
-        if at < span:
+        if chunked(at):
             for c in range(chunks):
                 outward(at, c).wait_send()
         else:
             outward(at).wait_send()
-        for p in range(pieces):
-            homeward(at, p).wait_send()
+
+    for p in range(pieces):
+        for at in range(n_sp):
+            if at != half:
+                homeward(at, p).wait_recv()
+        result = mixed[:, wide(p)].astype(F32)
+        for k in range(top):
+            result = result + scales[k] * jnp.dot(
+                picks[k], returned[:, wide(p)], preferred_element_type=F32
+            )
+        out_here[:, wide(p)] = result.astype(BF16)
+        out_copy(p).start()
+
+    for p in range(pieces):
+        for at in range(n_sp):
+            if at != half:
+                homeward(at, p).wait_send()
+        out_copy(p).wait()
 
 
 def per_device(
@@ -457,8 +571,8 @@
     return pl.pallas_call(
         functools.partial(kernel, n_sp, n_tp, quarter, capacity, top),
         out_shape=jax.ShapeDtypeStruct((quarter, width), BF16),
-        in_specs=[vmem] * 5 + [hbm] + [vmem] * 3 + [hbm] * 3,
-        out_specs=vmem,
+        in_specs=[hbm, vmem, vmem, hbm, vmem, hbm] + [vmem] * 3 + [hbm] * 3,
+        out_specs=hbm,
         scratch_shapes=[
             V((width, 2 * ff), BF16),
             V((width, 2 * ff), BF16),
@@ -480,8 +594,13 @@
             V((n_chip - 1, slots, 2 * ff), BF16),
             V((slots, width), BF16),
             V((slots, width), BF16),
+            V((n_chip - 1, quarter, width), BF16),
+            V((n_chip - 1, n_sp // 2 * capacity, width), BF16),
             V((rows, 128), F32),
-            dma((4,)),
+            V((group_width, branch_width), BF16),
+            V((quarter, width), BF16),
+            V((quarter, width), BF16),
+            dma((6,)),
             dma((2,)),
             dma((2,)),
             dma((2,)),
@@ -496,12 +615,17 @@
             dma((n_chip, chunks)),
             dma((n_sp, chunks)),
             dma((n_sp, chunks)),
-            dma((n_chip, 4)),
-            dma((n_chip, 4)),
+            dma((n_chip, 2)),
+            dma((n_chip, 2)),
             dma((n_chip, 4)),
             dma((n_chip, 4)),
             dma((n_sp, pieces)),
             dma((n_sp, pieces)),
+            dma((pieces,)),
+            dma((n_chip, chunks)),
+            dma((n_chip, chunks)),
+            dma((n_chip, n_sp)),
+            dma((n_chip, n_sp)),
         ],
         compiler_params=pltpu.CompilerParams(
             collective_id=0, has_side_effects=True, vmem_limit_bytes=60 * 1024 * 1024

time: 109 us -> 102 us (0.936)
  Pallas kernels: 107 us -> 100 us
    pallas_call x1, Pallas kernels: 107 us -> 100 us  [per_device(): pl.pallas_call(functools.partial(kernel, n_sp, n_tp, quarter, capacity, t...]
where the time goes in v1:
time: 102 us
  Pallas kernels  100 us (98%)
  local copies, waits for them, and re-layouts  1.88 us (2%)
    pallas_call x1, Pallas kernels, per_device(): pl.pallas_call(functools.partial(kernel, n_sp, n_tp, quarter, capacity, t...  100 us

profile of v1, /device:TPU:0, one launch (start us, length us, event | category | flops | bytes accessed | tf_op | source)
XLA Modules:
  0.0 102.2 jit_solution(12213674648715800903)
XLA Ops:
  0.0 100.3 %shard_map.118 = bf16[128,2048]{1,0:T(8,128)(2,1)} custom-call(bf16[128,2048]{1,0:T(8,128)(2,1)} %stream.1, bf16[512,256]{1,0:T(8,128)(2,1)} %pool_in.1, s32[1,512]{1,0:T(1,128)} %bitcast.15, bf16[256,512]{1,0:T(8,128)(2,1)} %bitcast.12, f32[1,512]{1,0:T(1,128)} %bitcast.16, bf16[512,2048]{1,0:T(8,128)(2,1)} %out_weight.1, f32[1,2048]{1,0:T(1,128)} %bitcast.13, ...), custom_call_target="tpu_custom_call" | custom-call | tf_op jit(solution)/shard_map/pallas_call | solution.py:571
  100.3 1.9 %copy.14 = bf16[128,2048]{1,0:T(8,128)(2,1)} copy(bf16[128,2048]{1,0:T(8,128)(2,1)} %shard_map.118) | data formatting | bytes 1048576

commit v2 on v1

--- a/solution.py
+++ b/solution.py
@@ -163,7 +163,7 @@
             for m in others:
                 far_down(p, m).start()
 
-    send_down(0, 1)
+    send_down(0)
 
     window = jnp.left_shift(jnp.int32(2), tp)
     group_width = pool_in.shape[1]
@@ -229,7 +229,7 @@
                 partial[owned(same(m)), cols(c)] + pair_recv[m, :, cols(c)].astype(F32)
             ).astype(BF16)
             far_copy(m, c).start()
-    send_down(2)
+    send_down(1, 2)
     for c in near_hidden:
         c.start()
     for p in range(pieces):
@@ -462,33 +462,34 @@
     far_hidden(0)
     send_down(4)
     normalize(1)
-    send_down(5)
     own_hidden(1)
     answer(0, 0, 1, 2)
     pass_down(3)
     answer(0, 3)
+    far_hidden(2)
+    pass_down(4)
+    answer(0, 4)
     normalize(3)
     own_hidden(3)
-    far_hidden(2)
     far_hidden(1)
+    send_down(5, 6, 7)
     far_hidden(3)
-    send_down(6, 7)
-    pass_down(4)
-    answer(0, 4)
     answer(1, 0, 1, 2, 3, 4)
     pass_down(5)
+    answer(2, 0, 1, 2, 3, 4)
     answer(0, 5)
     answer(1, 5)
-    answer(2, 0, 1, 2, 3, 4, 5)
     pass_down(6)
+    answer(2, 5)
+    answer(3, 0, 1, 2)
     answer(0, 6)
     answer(1, 6)
-    answer(3, 0, 1, 2, 3, 4, 5, 6)
     pass_down(7)
+    answer(3, 3, 4, 5)
     answer(0, 7)
     answer(1, 7)
     answer(2, 6, 7)
-    answer(3, 7)
+    answer(3, 6, 7)
 
     def out_copy(p):
         return pltpu.make_async_copy(
@@ -540,11 +541,11 @@
             )
         out_here[:, wide(p)] = result.astype(BF16)
         out_copy(p).start()
-
-    for p in range(pieces):
         for at in range(n_sp):
             if at != half:
                 homeward(at, p).wait_send()
+
+    for p in range(pieces):
         out_copy(p).wait()
 
 

time: 102 us -> 101 us (level)
  Pallas kernels: 100 us -> 98.7 us
    pallas_call x1, Pallas kernels: 100 us -> 98.7 us  [per_device(): pl.pallas_call(functools.partial(kernel, n_sp, n_tp, quarter, capacity, t...]
where the time goes in v2:
time: 101 us
  Pallas kernels  98.7 us (98%)
  local copies, waits for them, and re-layouts  1.88 us (2%)
    pallas_call x1, Pallas kernels, per_device(): pl.pallas_call(functools.partial(kernel, n_sp, n_tp, quarter, capacity, t...  98.7 us

profile of v2, /device:TPU:0, one launch (start us, length us, event | category | flops | bytes accessed | tf_op | source)
XLA Modules:
  0.0 100.6 jit_solution(5570221200287908907)
XLA Ops:
  0.0 98.7 %shard_map.118 = bf16[128,2048]{1,0:T(8,128)(2,1)} custom-call(bf16[128,2048]{1,0:T(8,128)(2,1)} %stream.1, bf16[512,256]{1,0:T(8,128)(2,1)} %pool_in.1, s32[1,512]{1,0:T(1,128)} %bitcast.15, bf16[256,512]{1,0:T(8,128)(2,1)} %bitcast.12, f32[1,512]{1,0:T(1,128)} %bitcast.16, bf16[512,2048]{1,0:T(8,128)(2,1)} %out_weight.1, f32[1,2048]{1,0:T(1,128)} %bitcast.13, ...), custom_call_target="tpu_custom_call" | custom-call | tf_op jit(solution)/shard_map/pallas_call | solution.py:572
  98.7 1.9 %copy.14 = bf16[128,2048]{1,0:T(8,128)(2,1)} copy(bf16[128,2048]{1,0:T(8,128)(2,1)} %shard_map.118) | data formatting | bytes 1048576
